TPU v7x, 512 devices: a whole 4x4x16 slice. The times are simulated.
512 devices in a mesh: fs: 64 (over z, y), tp: 8 (over x, core).
Axes of the slice: x: 4, y: 4, z: 16, core: 2. Of those that a mesh axis runs over, the one named last changes fastest.
Arguments:
- inputs: bfloat16 [16384, 2048], P('fs'), may hold values from -6 to 6
- query_cot: bfloat16 [16384, 1024], P('fs', 'tp'), may hold values from -0.046875 to 0.046875
- query_basis: bfloat16 [2048, 256], P('fs'), may hold values from -0.125 to 0.125
- query_master: float32 [2048, 1024], P('fs', 'tp'), may hold values from -3 to 3
- query_first: float32 [256, 1024], P('fs', 'tp'), may hold values from -4 to 4
- query_second: float32 [256, 1024], P('fs', 'tp'), may hold values from 0.02 to 4
Outputs:
- query_step: float32 [2048, 1024], P('fs', 'tp')
- query_first_new: float32 [256, 1024], P('fs', 'tp')
- query_second_new: float32 [256, 1024], P('fs', 'tp')
- query_copy: bfloat16 [2048, 1024], P('fs', 'tp')
All inputs are finite; a program needn't handle non-finite values.
Results may differ from a plain program's by a relative error of at most 0.0011.
Values may be sent and summed in bfloat16 or wider, within the bound.
A program may use at most 64 MiB of HBM per device.

v0:
```python
import jax
import jax.numpy as jnp
from jax import lax
from jax.sharding import Mesh
from jax.sharding import PartitionSpec as P

HEADS = 8
DQK = 128
RANK = 256
TP = ("tp_0", "tp_1")
FS = ("fs_0", "fs_1")
FS_TP = ("fs_0", "fs_1", "tp_0", "tp_1")


CONTRACT = (((0,), (0,)), ((), ()))


def in_blocks(shard, dim, devices):
    before, after = (shard.shape[:dim], shard.shape[dim + 1 :])
    return jnp.moveaxis(shard.reshape(*before, devices, -1, *after), dim, 0)


def summed_on_arrival(shard, axis, dim):
    devices = lax.axis_size(axis)
    parts = lax.all_to_all(in_blocks(shard, dim, devices), axis, 0, 0, tiled=True)
    return jnp.sum(parts, axis=0)


def one_axis_at_a_time(shard, axes):
    for axis in axes:
        shard = lax.psum(shard, axis)
    return shard


def in_order(parts, dim):
    lengths = list(parts.shape[1:])
    lengths[dim] *= parts.shape[0]
    return jnp.moveaxis(parts, 0, dim).reshape(lengths)


def copy_for_each(shard, axis):
    copies = jnp.broadcast_to(shard, (lax.axis_size(axis), *shard.shape))
    return lax.all_to_all(copies, axis, split_axis=0, concat_axis=0, tiled=True)


def collect(shard, axis, dim):
    return in_order(copy_for_each(shard, axis), dim)


def moments(first, second, low_grad):
    first_new = 0.8 * first + 0.2 * low_grad
    second_new = 0.9 * second + 0.1 * low_grad * low_grad
    return (first_new, second_new, first_new / jnp.sqrt(second_new))


def head_sums(update, width):
    heads_local = update.shape[1] // width
    squares = jnp.sum((update * update).reshape(-1, heads_local, width), axis=(0, 2))
    offset = lax.axis_index(TP) * heads_local
    return lax.dynamic_update_slice(jnp.zeros((HEADS,), jnp.float32), squares, (offset,))


def apply_scale(update, totals, width):
    heads_local = update.shape[1] // width
    offset = lax.axis_index(TP) * heads_local
    head_mean = lax.dynamic_slice(totals, (offset,), (heads_local,)) / (RANK * width)
    whole_mean = jnp.sum(totals) / (RANK * HEADS * width)
    factor = 1.0 / jnp.sqrt(head_mean + whole_mean)
    return (update.reshape(-1, heads_local, width) * factor[None, :, None]).reshape(update.shape)


def body(inputs, query_cot, query_basis, query_master, query_first, query_second):
    basis_q = query_basis.astype(jnp.float32)
    gradient = summed_on_arrival(
        lax.dot_general(inputs, query_cot, CONTRACT, preferred_element_type=jnp.float32), FS, 0
    )
    low_parts = summed_on_arrival(
        lax.dot_general(basis_q, gradient, CONTRACT, precision=lax.Precision.HIGHEST), FS, 0
    )
    first_q, second_q, update_q = moments(query_first, query_second, low_parts)
    totals_q = one_axis_at_a_time(head_sums(update_q, DQK), FS_TP)
    scaled_q = apply_scale(update_q, totals_q, DQK)
    gathered_q = collect(scaled_q, FS, 0)
    step_q = jnp.dot(basis_q, gathered_q, precision=lax.Precision.HIGHEST)
    copy_q = (query_master + step_q).astype(jnp.bfloat16)
    return (step_q, first_q, second_q, copy_q)


def solution(mesh):
    torus = Mesh(mesh.devices.reshape(16, 4, 4, 2), ("fs_0", "fs_1", "tp_0", "tp_1"))
    in_specs = (P(FS, None), P(FS, TP), P(FS, None), P(FS, TP), P(FS, TP), P(FS, TP))
    out_specs = (P(FS, TP), P(FS, TP), P(FS, TP), P(FS, TP))
    return jax.shard_map(body, mesh=torus, in_specs=in_specs, out_specs=out_specs, check_vma=False)
```

profile of v0, /device:TPU:1, one launch (start us, length us, event | category | flops | bytes accessed | tf_op | source)
XLA Modules:
  0.0 177.7 jit_solution(7039905519884814700)
XLA Ops:
  0.6 0.0 copy-start
  0.6 1.2 copy-done
  1.9 1.3 fusion.2
  3.2 70.7 %all_to_all.15 = f32[64,32,128]{2,1,0:T(8,128)S(1)} all-to-all(f32[64,32,128]{2,1,0:T(8,128)S(1)} %bitcast.16), channel_id=1, replica_groups=mesh['fs_0'=16,'fs_1'=4,'tp_0'=4,'tp_1'=2] {'fs_0','fs_1'}, dimensions={0} | all-to-all | bytes 2097152 | tf_op jit(solution)/shard_map/all_to_all | solution.py:25
  73.9 0.0 copy-start.1
  73.9 0.1 reduce_sum.38
  74.0 0.6 copy-done.1
  74.6 0.3 convolution_bitcast_fusion
  74.9 0.7 copy.10
  75.6 8.6 %all-to-all-start.1 = ((f32[64,4,128]{2,1,0:T(4,128)}), f32[64,4,128]{2,1,0:T(4,128)S(1)}, u32[]{:S(2)}, u32[]{:S(2)}) async-start(f32[64,4,128]{2,1,0:T(4,128)} %bitcast.2), calls=%async_computation.1 | async-start | bytes 262144 | tf_op jit(solution)/shard_map/all_to_all | solution.py:25
  84.2 0.0 copy-start.5
  84.2 0.0 copy-start.6
  84.2 15.0 %all-to-all-done.1 = f32[64,4,128]{2,1,0:T(4,128)S(1)} async-done(((f32[64,4,128]{2,1,0:T(4,128)}), f32[64,4,128]{2,1,0:T(4,128)S(1)}, u32[]{:S(2)}, u32[]{:S(2)}) %all-to-all-start.1) | async-done | bytes 131104 | tf_op jit(solution)/shard_map/all_to_all | solution.py:25
  99.2 0.1 reduce_sum.39
  99.3 0.0 copy-done.5
  99.3 0.0 copy-done.6
  99.3 0.6 multiply_reduce_fusion
  99.9 0.0 copy-start.3
  99.9 0.0 copy-start.4
  99.9 0.8 dynamic_update_slice.3
  100.7 20.5 %psum.28 = f32[8]{0:T(128)S(1)} all-reduce(f32[8]{0:T(128)S(1)} %dynamic_update_slice.3), channel_id=1, replica_groups=mesh['fs_0'=16,'fs_1'=4,'tp_0'=4,'tp_1'=2] {'fs_0'}, use_global_device_ids=true, to_apply=%region_3.0 | all-reduce | flops 8 | bytes 64 | tf_op jit(solution)/shard_map/psum | solution.py:31
  121.2 7.4 %psum.29 = f32[8]{0:T(128)S(1)} all-reduce(f32[8]{0:T(128)S(1)} %psum.28), channel_id=1, replica_groups=mesh['fs_0'=16,'fs_1'=4,'tp_0'=4,'tp_1'=2] {'fs_1'}, use_global_device_ids=true, to_apply=%region_4.0 | all-reduce | flops 8 | bytes 64 | tf_op jit(solution)/shard_map/psum | solution.py:31
  128.6 8.5 %psum.30 = f32[8]{0:T(128)S(1)} all-reduce(f32[8]{0:T(128)S(1)} %psum.29), channel_id=1, replica_groups=mesh['fs_0'=16,'fs_1'=4,'tp_0'=4,'tp_1'=2] {'tp_0'}, use_global_device_ids=true, to_apply=%region_5.0 | all-reduce | flops 8 | bytes 64 | tf_op jit(solution)/shard_map/psum | solution.py:31
  137.1 16.3 %psum.31 = f32[8]{0:T(128)S(1)} all-reduce(f32[8]{0:T(128)S(1)} %psum.30), channel_id=1, replica_groups=mesh['fs_0'=16,'fs_1'=4,'tp_0'=4,'tp_1'=2] {'tp_1'}, use_global_device_ids=true, to_apply=%region_6.0 | all-reduce | flops 8 | bytes 64 | tf_op jit(solution)/shard_map/psum | solution.py:31
  153.4 0.6 dynamic_slice.3
  154.0 0.6 reduce_sum.42
  155.9 0.0 copy-done.3
  155.9 0.0 copy-done.4
  156.0 0.0 copy-start.2
  156.0 20.9 %all_to_all.16 = f32[64,4,128]{2,1,0:T(4,128)S(1)} all-to-all(f32[64,4,128]{2,1,0:T(4,128)S(1)} %broadcast_in_dim.4), channel_id=1, replica_groups=mesh['fs_0'=16,'fs_1'=4,'tp_0'=4,'tp_1'=2] {'fs_0','fs_1'}, dimensions={0} | all-to-all | bytes 262144 | tf_op jit(solution)/shard_map/all_to_all | solution.py:43
  176.9 0.0 copy-done.2
  176.9 0.8 add_convert_fusion
  (3 shorter events, 0.0 us)
Async XLA Ops:
  0.6 1.2 copy-start
  73.9 0.7 copy-start.1
  75.6 23.6 %all-to-all-start.1 = ((f32[64,4,128]{2,1,0:T(4,128)}), f32[64,4,128]{2,1,0:T(4,128)S(1)}, u32[]{:S(2)}, u32[]{:S(2)}) async-start(f32[64,4,128]{2,1,0:T(4,128)} %bitcast.2), calls=%async_computation.1 | async-start | bytes 262144 | tf_op jit(solution)/shard_map/all_to_all | solution.py:25
  84.2 15.1 %copy-start.5 = (f32[4,128]{1,0:T(4,128)S(1)}, f32[4,128]{1,0:T(4,128)}, u32[]{:S(2)}) copy-start(f32[4,128]{1,0:T(4,128)} %param.11) | copy-start | bytes 6148
  84.2 15.1 %copy-start.6 = (f32[4,128]{1,0:T(4,128)S(1)}, f32[4,128]{1,0:T(4,128)}, u32[]{:S(2)}) copy-start(f32[4,128]{1,0:T(4,128)} %param.10) | copy-start | bytes 6148
  99.9 56.0 %copy-start.3 = (f32[4,128]{1,0:T(4,128)}, f32[4,128]{1,0:T(4,128)S(1)}, u32[]{:S(2)}) copy-start(f32[4,128]{1,0:T(4,128)S(1)} %get-tuple-element.5) | copy-start | bytes 6148
  99.9 56.0 %copy-start.4 = (f32[4,128]{1,0:T(4,128)}, f32[4,128]{1,0:T(4,128)S(1)}, u32[]{:S(2)}) copy-start(f32[4,128]{1,0:T(4,128)S(1)} %get-tuple-element.6) | copy-start | bytes 6148
  156.0 20.9 %copy-start.2 = (f32[32,128]{1,0:T(8,128)S(1)}, f32[32,128]{1,0:T(8,128)}, u32[]{:S(2)}) copy-start(f32[32,128]{1,0:T(8,128)} %param.9) | copy-start | bytes 49156
where the time goes:
time: 179 us; the launch traced here: 178 us
  blocking collectives  144 us (80%)
  waiting for transfers between devices  15 us (8%)
  starting transfers between devices  8.58 us (5%)
  local copies, waits for them, and re-layouts  3.97 us (2%)
  matrix products  2.37 us (1%)
  between operations  2.07 us (1%)
    all_to_all x1, blocking collectives, summed_on_arrival(): lax.all_to_all(in_blocks(shard, dim, devices), axis, 0, 0, tiled=True)  70.7 us
    psum x4, blocking collectives, one_axis_at_a_time(): shard = lax.psum(shard, axis)  52.7 us
    all_to_all x1, blocking collectives, copy_for_each(): return lax.all_to_all(copies, axis, split_axis=0, concat_axis=0, tiled=True)  20.9 us
    all_to_all x1, waiting for transfers between devices, summed_on_arrival(): lax.all_to_all(in_blocks(shard, dim, devices), axis, 0, 0, tiled=True)  15 us
    all_to_all x1, starting transfers between devices, summed_on_arrival(): lax.all_to_all(in_blocks(shard, dim, devices), axis, 0, 0, tiled=True)  8.58 us
  transfers between devices with their start and end apart: 1, of which 1 were waited for; matrix products, arithmetic and copies ran while one was open for 0% of the time, Pallas kernels for 0%

commit v1 on v0

v1 whole, which is shorter than its diff:
```python
import jax
import jax.numpy as jnp
from jax import lax
from jax.experimental import pallas as pl
from jax.experimental.pallas import tpu as pltpu
from jax.sharding import Mesh
from jax.sharding import PartitionSpec as P

HEADS = 8
DQK = 128
RANK = 256
NZ, NY, NX, NC = 16, 4, 4, 2
NF, NT = NZ * NY, NX * NC
TP = ("x", "c")
FS = ("z", "y")
MESH = pl.DeviceIdType.MESH


def far_first(k, n):
    h = (k + 1) // 2
    return lax.rem(n // 2 + h * (1 - 2 * lax.rem(k, 2)) + n, n)


def moments(first, second, low_grad):
    first_new = 0.8 * first + 0.2 * low_grad
    second_new = 0.9 * second + 0.1 * low_grad * low_grad
    return (first_new, second_new, first_new / jnp.sqrt(second_new))


def kernel(x_hbm, c_hbm, b_hbm, first_hbm, second_hbm, out_ref,
           x_v, c_v, b_v, first_v, second_v, p_v, s_v, r_v, u_v, t_v, g_v,
           local_sem, send_sem, recv_sem):
    z, y, x, c = (lax.axis_index(a) for a in ("z", "y", "x", "c"))
    f, s = z * NY + y, x * NC + c

    def fs_peer(j):
        return (lax.rem(z + far_first(j // NY, NZ), NZ), lax.rem(y + far_first(lax.rem(j, NY), NY), NY), x, c)

    def tp_peer(j):
        t = lax.rem(s + 1 + j, NT)
        return (z, y, t // NC, lax.rem(t, NC))

    def each(n, do):
        def step(j, carry):
            do(j)
            return carry
        lax.fori_loop(0, n, step, 0)

    def remote(src, dst, phase, peer):
        return pltpu.make_async_remote_copy(src_ref=src, dst_ref=dst, send_sem=send_sem.at[phase],
                                            recv_sem=recv_sem.at[phase], device_id=peer, device_id_type=MESH)

    def wait_for(window, sem):
        pltpu.make_async_copy(window, window, sem).wait()

    barrier = pltpu.get_barrier_semaphore()
    each(NF - 1, lambda j: pl.semaphore_signal(barrier, inc=1, device_id=fs_peer(j), device_id_type=MESH))
    each(NT - 1, lambda j: pl.semaphore_signal(barrier, inc=1, device_id=tp_peer(j), device_id_type=MESH))

    mine = pl.ds(pl.multiple_of(s * DQK, DQK), DQK)
    loads = [pltpu.make_async_copy(src, dst, local_sem.at[i]) for i, (src, dst) in enumerate((
        (b_hbm, b_v), (c_hbm, c_v.at[:, mine]), (x_hbm, x_v), (first_hbm, first_v), (second_hbm, second_v)))]
    for load in loads:
        load.start()

    lane = lax.broadcasted_iota(jnp.int32, (RANK, 128), 1)
    row = lax.broadcasted_iota(jnp.int32, (RANK, 128), 0)
    slot = lane & 31
    to_z = 2 * (slot >> 2) + c
    chosen = row == 16 * to_z + 4 * ((to_z + x) & 3) + (slot & 3)
    select = jnp.where(chosen, 1.0, 0.0).astype(jnp.bfloat16)
    group = lax.broadcasted_iota(jnp.int32, (8, 128), 1) >> 5
    loads[0].wait()
    picked = jnp.dot(b_v[...], select, preferred_element_type=jnp.float32)
    packed = jnp.zeros((8, 128), jnp.float32)
    for j in range(4):
        packed = jnp.where(group == j, picked[8 * j : 8 * j + 8], packed)
    p_v[f] = packed.astype(jnp.bfloat16)
    loads[1].wait()

    pl.semaphore_wait(barrier, NF - 1 + NT - 1)
    each(NF - 1, lambda j: remote(p_v.at[f], p_v.at[f], 0, fs_peer(j)).start())
    each(NT - 1, lambda j: remote(c_v.at[:, mine], c_v.at[:, mine], 1, tp_peer(j)).start())
    for load in loads[2:]:
        load.wait()
    wait_for(p_v.at[pl.ds(0, NF - 1)], recv_sem.at[0])

    blocks = p_v[...].astype(jnp.float32)
    which = lax.broadcasted_iota(jnp.int32, (NF, 4, 8, 128), 1)
    lanes = lax.broadcasted_iota(jnp.int32, (NF, 4, 8, 128), 3) >> 5
    spread = jnp.where(which == lanes, blocks[:, None], 0.0).reshape(NF * 32, 128).astype(jnp.bfloat16)
    wide = jnp.dot(x_v[...], spread, preferred_element_type=jnp.float32).T
    proj = wide[0:32] + wide[32:64] + wide[64:96] + wide[96:128]
    high = proj.astype(jnp.bfloat16)
    rest = (proj - high.astype(jnp.float32)).astype(jnp.bfloat16)
    both = jnp.concatenate([high, rest], axis=0)
    wait_for(c_v.at[:, pl.ds(0, (NT - 1) * DQK)], recv_sem.at[1])
    part = jnp.dot(both, c_v[...], preferred_element_type=jnp.float32)
    part = part[:32] + part[32:]
    for k in range(8):
        for t in range(NT):
            s_v[k, t] = part[4 * k : 4 * k + 4, DQK * t : DQK * (t + 1)]

    own = jnp.logical_and(lax.rem(z, 2) == c, lax.rem(z + x, NY) == y)

    def send_part(j):
        k = lax.rem(z // 2 + far_first(j // NT, 8), 8)
        to_z = 2 * k + c
        to_y = lax.rem(to_z + x, NY)
        t = lax.rem(s + 1 + lax.rem(j, NT), NT)
        here = jnp.logical_and(jnp.logical_and(to_z == z, to_y == y), t == s)

        @pl.when(here)
        def _():
            pltpu.make_async_copy(s_v.at[k, t], r_v.at[f], recv_sem.at[2]).start()

        @pl.when(jnp.logical_not(here))
        def _():
            remote(s_v.at[k, t], r_v.at[f], 2, (to_z, to_y, t // NC, lax.rem(t, NC))).start()

    each(NF, send_part)
    wait_for(r_v, recv_sem.at[2])

    low = jnp.sum(r_v[...], axis=0)
    update = moments(first_v[...], second_v[...], low)[2]
    u_v[f] = update
    t_v[s] = jnp.sum(update * update, axis=0, keepdims=True)
    each(NT - 1, lambda j: remote(t_v.at[s], t_v.at[s], 3, tp_peer(j)).start())
    each(NF - 1, lambda j: remote(u_v.at[f], u_v.at[f], 4, fs_peer(j)).start())
    wait_for(t_v.at[pl.ds(0, NT - 1)], recv_sem.at[3])
    g_v[f] = jnp.sum(t_v[...], axis=0)
    each(NF - 1, lambda j: remote(g_v.at[f], g_v.at[f], 5, fs_peer(j)).start())
    wait_for(u_v.at[pl.ds(0, NF - 1)], recv_sem.at[4])

    whole = u_v[...].reshape(RANK, DQK)
    head_mean = jnp.sum(whole * whole) / (RANK * DQK)
    high = whole.astype(jnp.bfloat16)
    rest = whole - high.astype(jnp.float32)
    middle = rest.astype(jnp.bfloat16)
    least = (rest - middle.astype(jnp.float32)).astype(jnp.bfloat16)
    basis = b_v[...]
    raw = (jnp.dot(basis, high, preferred_element_type=jnp.float32)
           + (jnp.dot(basis, middle, preferred_element_type=jnp.float32)
              + jnp.dot(basis, least, preferred_element_type=jnp.float32)))
    wait_for(g_v.at[pl.ds(0, NF - 1)], recv_sem.at[5])
    whole_mean = jnp.sum(g_v[...]) / (RANK * HEADS * DQK)
    out_ref[0:32] = raw
    out_ref[32:36] = low
    out_ref[36:40] = jnp.full((4, DQK), head_mean + whole_mean, jnp.float32)

    wait_for(p_v.at[pl.ds(0, NF - 1)], send_sem.at[0])
    wait_for(c_v.at[:, pl.ds(0, (NT - 1) * DQK)], send_sem.at[1])

    @pl.when(own)
    def _():
        wait_for(r_v.at[pl.ds(0, NF - 1)], send_sem.at[2])

    @pl.when(jnp.logical_not(own))
    def _():
        wait_for(r_v, send_sem.at[2])

    wait_for(t_v.at[pl.ds(0, NT - 1)], send_sem.at[3])
    wait_for(u_v.at[pl.ds(0, NF - 1)], send_sem.at[4])
    wait_for(g_v.at[pl.ds(0, NF - 1)], send_sem.at[5])


def body(inputs, query_cot, query_basis, query_master, query_first, query_second):
    bf16, f32 = jnp.bfloat16, jnp.float32
    out = pl.pallas_call(
        kernel,
        out_shape=jax.ShapeDtypeStruct((40, DQK), f32),
        in_specs=[pl.BlockSpec(memory_space=pl.ANY)] * 5,
        out_specs=pl.BlockSpec(memory_space=pltpu.VMEM),
        scratch_shapes=[
            pltpu.VMEM((256, 2048), bf16),
            pltpu.VMEM((256, NT * DQK), bf16),
            pltpu.VMEM((32, RANK), bf16),
            pltpu.VMEM((4, DQK), f32),
            pltpu.VMEM((4, DQK), f32),
            pltpu.VMEM((NF, 8, 128), bf16),
            pltpu.VMEM((8, NT, 4, DQK), f32),
            pltpu.VMEM((NF, 4, DQK), f32),
            pltpu.VMEM((NF, 4, DQK), f32),
            pltpu.VMEM((NT, 1, DQK), f32),
            pltpu.VMEM((NF, 1, DQK), f32),
            pltpu.SemaphoreType.DMA((5,)),
            pltpu.SemaphoreType.DMA((6,)),
            pltpu.SemaphoreType.DMA((6,)),
        ],
        compiler_params=pltpu.CompilerParams(collective_id=0, has_side_effects=True),
    )(inputs, query_cot, query_basis, query_first, query_second)
    factor = 1.0 / jnp.sqrt(out[36:37])
    step_q = out[0:32] * factor
    first_q, second_q, _ = moments(query_first, query_second, out[32:36])
    copy_q = (query_master + step_q).astype(bf16)
    return (step_q, first_q, second_q, copy_q)


def solution(mesh):
    torus = Mesh(mesh.devices.reshape(NZ, NY, NX, NC), ("z", "y", "x", "c"))
    in_specs = (P(FS, None), P(FS, TP), P(FS, None), P(FS, TP), P(FS, TP), P(FS, TP))
    out_specs = (P(FS, TP), P(FS, TP), P(FS, TP), P(FS, TP))
    return jax.shard_map(body, mesh=torus, in_specs=in_specs, out_specs=out_specs, check_vma=False)
```

time: 179 us -> 57.9 us (0.32)
  blocking collectives: 144 us -> 0 us
  Pallas kernels: 0 us -> 52.9 us
  waiting for transfers between devices: 15 us -> 0 us
  starting transfers between devices: 8.58 us -> 0 us
  local copies, waits for them, and re-layouts: 3.97 us -> 1.38 us
  matrix products: 2.37 us -> 0 us
    all_to_all x2 -> x0, blocking collectives: 91.6 us -> none  [the longest x1 70.7 us: summed_on_arrival(): lax.all_to_all(in_blocks(shard, dim, devices), axis, 0, 0, tiled=True)]
    pallas_call x0 -> x1, Pallas kernels: none -> 52.9 us  [body(): pl.pallas_call(kernel, out_shape=jax.ShapeDtypeStruct((40, DQK), f32), in...]
    psum x4 -> x0, blocking collectives: 52.7 us -> none  [one_axis_at_a_time(): shard = lax.psum(shard, axis)]
    all_to_all x1 -> x0, waiting for transfers between devices: 15 us -> none  [summed_on_arrival(): lax.all_to_all(in_blocks(shard, dim, devices), axis, 0, 0, tiled=True)]
    all_to_all x1 -> x0, starting transfers between devices: 8.58 us -> none  [summed_on_arrival(): lax.all_to_all(in_blocks(shard, dim, devices), axis, 0, 0, tiled=True)]
    dot_general x3 -> x0, matrix products: 2.37 us -> none  [the longest x1 1.33 us: body(): lax.dot_general(inputs, query_cot, CONTRACT, preferred_element_type=jnp.f...]
  transfers between devices with their start and end apart: 1 -> 0, of which waited for: 1 -> 0; matrix products, arithmetic and copies ran while one was open for 0% -> 0% of each run, Pallas kernels for 0% -> 0%
where the time goes in v1:
time: 57.9 us; the launch traced here: 57.5 us
  Pallas kernels  52.9 us (91%)
  other arithmetic  2.62 us (5%)
  local copies, waits for them, and re-layouts  1.38 us (2%)
  between operations  0.65 us (1%)
    pallas_call x1, Pallas kernels, body(): pl.pallas_call(kernel, out_shape=jax.ShapeDtypeStruct((40, DQK), f32), in...  52.9 us
    convert_element_type x1, other arithmetic, body(): copy_q = (query_master + step_q).astype(bf16)  1.34 us
    add x1, other arithmetic, moments(): second_new = 0.9 * second + 0.1 * low_grad * low_grad  1.27 us

profile of v1, /device:TPU:1, one launch (start us, length us, event | category | flops | bytes accessed | tf_op | source)
XLA Modules:
  0.0 57.5 jit_solution(5638675801159944945)
XLA Ops:
  0.6 0.0 copy-start
  0.6 52.9 %shard_map.93 = f32[40,128]{1,0:T(8,128)} custom-call(bf16[256,2048]{1,0:T(8,128)(2,1)} %x_hbm.1, bf16[256,128]{1,0:T(8,128)(2,1)} %c_hbm.1, bf16[32,256]{1,0:T(8,128)(2,1)} %b_hbm.1, f32[4,128]{1,0:T(4,128)} %first_hbm.1, f32[4,128]{1,0:T(4,128)} %second_hbm.1), custom_call_target="tpu_custom_call" | custom-call | tf_op jit(solution)/shard_map/pallas_call | solution.py:169
  53.5 0.7 %rsqrt_bitcast_fusion = f32[128]{0:T(128)S(1)} fusion(f32[40,128]{1,0:T(8,128)} %shard_map.93), kind=kLoop, calls=%fused_computation.5 | loop fusion | bytes 1024 | tf_op jit(solution)/shard_map/mul | solution.py:193
  54.2 0.0 copy-done
  54.2 0.0 copy-start.2
  54.2 1.3 %add_convert_fusion = (bf16[32,128]{1,0:T(8,128)(2,1)}, f32[32,128]{1,0:T(8,128)}) fusion(f32[32,128]{1,0:T(8,128)S(1)} %copy-done, f32[128]{0:T(128)S(1)} %rsqrt_bitcast_fusion, f32[40,128]{1,0:T(8,128)} %shard_map.93), kind=kLoop, calls=%fused_computation | loop fusion | flops 12288 | bytes 57856 | tf_op jit(solution)/shard_map/convert_element_type | solution.py:195
  55.6 0.0 copy-start.1
  55.6 0.0 copy-done.2
  55.6 0.7 %copy-done.1 = f32[4,128]{1,0:T(4,128)S(1)} copy-done((f32[4,128]{1,0:T(4,128)S(1)}, f32[4,128]{1,0:T(4,128)}, u32[]{:S(2)}) %copy-start.1) | copy-done | bytes 2072
  56.3 1.3 %fusion = (f32[4,128]{1,0:T(4,128)}, f32[4,128]{1,0:T(4,128)}) fusion(f32[4,128]{1,0:T(4,128)S(1)} %copy-done.2, f32[40,128]{1,0:T(8,128)} %shard_map.93, f32[4,128]{1,0:T(4,128)S(1)} %copy-done.1), kind=kLoop, calls=%fused_computation.3 | loop fusion | flops 3584 | bytes 10240 | tf_op jit(solution)/shard_map/add | solution.py:26
Async XLA Ops:
  0.6 53.6 %copy-start = (f32[32,128]{1,0:T(8,128)S(1)}, f32[32,128]{1,0:T(8,128)}, u32[]{:S(2)}) copy-start(f32[32,128]{1,0:T(8,128)} %param.9) | copy-start | bytes 49156
  54.2 1.4 %copy-start.2 = (f32[4,128]{1,0:T(4,128)S(1)}, f32[4,128]{1,0:T(4,128)}, u32[]{:S(2)}) copy-start(f32[4,128]{1,0:T(4,128)} %second_hbm.1) | copy-start | bytes 6148
  55.6 0.7 %copy-start.1 = (f32[4,128]{1,0:T(4,128)S(1)}, f32[4,128]{1,0:T(4,128)}, u32[]{:S(2)}) copy-start(f32[4,128]{1,0:T(4,128)} %first_hbm.1) | copy-start | bytes 6148

commit v2 on v1

v2 whole, which is shorter than its diff:
```python
import jax
import jax.numpy as jnp
from jax import lax
from jax.experimental import pallas as pl
from jax.experimental.pallas import tpu as pltpu
from jax.sharding import Mesh
from jax.sharding import PartitionSpec as P

HEADS = 8
DQK = 128
RANK = 256
NZ, NY, NX, NC = 16, 4, 4, 2
NF, NT = NZ * NY, NX * NC
TP = ("x", "c")
FS = ("z", "y")
MESH = pl.DeviceIdType.MESH
BASIS, UPDATE, PARTS, NEAR, LINE, CORE, CROSS = 0, 1, 2, 3, 4, 5, 6
Y_ORDER = (2, 1, 3, 0)


def moments(first, second, low_grad):
    first_new = 0.8 * first + 0.2 * low_grad
    second_new = 0.9 * second + 0.1 * low_grad * low_grad
    return (first_new, second_new, first_new / jnp.sqrt(second_new))


def kernel(x_hbm, c_hbm, b_hbm, first_hbm, second_hbm, out_ref,
           x_v, c_v, b_v, first_v, second_v, p_v, s_v, r_v, u_v, n_v, g_v,
           local_sem, send_sem, recv_sem):
    z, y, x, c = (lax.axis_index(a) for a in ("z", "y", "x", "c"))
    f, s = z * NY + y, x * NC + c
    asides = [lax.rem(y + d, NY) for d in Y_ORDER]
    places = [lax.rem(s + j, NT) for j in range(1, NT)] + [s]
    sides = [(lax.div(t, NC), lax.rem(t, NC)) for t in places]

    def to_fs(do):
        def ring(k, carry):
            h = lax.div(k + 1, 2)
            to_z = lax.rem(z + 8 + h * (1 - 2 * lax.rem(k, 2)), NZ)
            for to_y in asides:
                do((to_z, to_y, x, c))
            return carry
        lax.fori_loop(0, NZ - 1, ring, 0)
        for to_y in asides[:-1]:
            do((z, to_y, x, c))

    def to_tp(do):
        for to_x, to_c in sides[:-1]:
            do((z, y, to_x, to_c))

    def remote(src, dst, phase, peer):
        return pltpu.make_async_remote_copy(src_ref=src, dst_ref=dst, send_sem=send_sem.at[phase],
                                            recv_sem=recv_sem.at[phase], device_id=peer, device_id_type=MESH)

    def wait_for(window, sem):
        pltpu.make_async_copy(window, window, sem).wait()

    barrier = pltpu.get_barrier_semaphore()
    to_fs(lambda peer: pl.semaphore_signal(barrier, inc=1, device_id=peer, device_id_type=MESH))
    to_tp(lambda peer: pl.semaphore_signal(barrier, inc=1, device_id=peer, device_id_type=MESH))

    def columns(t):
        return c_v.at[:, pl.ds(pl.multiple_of(t * DQK, DQK), DQK)]

    loads = [pltpu.make_async_copy(src, dst, local_sem.at[i]) for i, (src, dst) in enumerate((
        (b_hbm, b_v), (c_hbm, columns(s)), (x_hbm, x_v), (first_hbm, first_v), (second_hbm, second_v)))]
    for load in loads:
        load.start()

    lane = lax.broadcasted_iota(jnp.int32, (RANK, 128), 1)
    row = lax.broadcasted_iota(jnp.int32, (RANK, 128), 0)
    slot = lane & 31
    to_z = 2 * (slot >> 2) + c
    chosen = row == 16 * to_z + 4 * ((to_z + x) & 3) + (slot & 3)
    select = jnp.where(chosen, 1.0, 0.0).astype(jnp.bfloat16)
    group = lax.broadcasted_iota(jnp.int32, (8, 128), 1) >> 5
    loads[0].wait()
    picked = jnp.dot(b_v[...], select, preferred_element_type=jnp.float32)
    packed = jnp.zeros((8, 128), jnp.float32)
    for j in range(4):
        packed = jnp.where(group == j, picked[8 * j : 8 * j + 8], packed)
    p_v[f] = packed.astype(jnp.bfloat16)
    for load in loads[1:]:
        load.wait()

    pl.semaphore_wait(barrier, NF - 1 + NT - 1)
    across = [lax.rem(x + d, NX) for d in (2, 1, 3)]
    partner = (z, y, x, 1 - c)
    for i, to_x in enumerate(across):
        remote(columns(s), columns(s), CROSS + i, (z, y, to_x, c)).start()
    remote(columns(s), columns(s), CORE, partner).start()
    to_fs(lambda peer: remote(p_v.at[f], p_v.at[f], BASIS, peer).start())
    for i in (1, 2, 0):
        came = columns(lax.rem(x + NX - (2, 1, 3)[i], NX) * NC + c)
        wait_for(came, recv_sem.at[CROSS + i])
        remote(came, came, CORE, partner).start()
    wait_for(p_v.at[pl.ds(0, NF - 1)], recv_sem.at[BASIS])

    blocks = p_v[...].astype(jnp.float32)
    which = lax.broadcasted_iota(jnp.int32, (NF, 4, 8, 128), 1)
    lanes = lax.broadcasted_iota(jnp.int32, (NF, 4, 8, 128), 3) >> 5
    spread = jnp.where(which == lanes, blocks[:, None], 0.0).reshape(NF * 32, 128).astype(jnp.bfloat16)
    wide = jnp.dot(x_v[...], spread, preferred_element_type=jnp.float32).T
    proj = wide[0:32] + wide[32:64] + wide[64:96] + wide[96:128]
    high = proj.astype(jnp.bfloat16)
    rest = (proj - high.astype(jnp.float32)).astype(jnp.bfloat16)
    both = jnp.concatenate([high, rest], axis=0)
    wait_for(c_v.at[:, pl.ds(0, NX * DQK)], recv_sem.at[CORE])
    part = jnp.dot(both, c_v[...], preferred_element_type=jnp.float32)
    part = part[:32] + part[32:]
    for k in range(8):
        for t in range(NT):
            s_v[k, t] = part[4 * k : 4 * k + 4, DQK * t : DQK * (t + 1)]

    own = jnp.logical_and(lax.rem(z, 2) == c, lax.rem(z + x, NY) == y)

    def send_parts(j, carry):
        h = lax.div(j + 1, 2)
        k = lax.rem(lax.div(z, 2) + 4 + h * (1 - 2 * lax.rem(j, 2)), 8)
        to_z = 2 * k + c
        to_y = lax.rem(to_z + x, NY)
        for t, (to_x, to_c) in zip(places[:-1], sides):
            remote(s_v.at[k, t], r_v.at[f], PARTS, (to_z, to_y, to_x, to_c)).start()
        here = jnp.logical_and(to_z == z, to_y == y)

        @pl.when(here)
        def _():
            pltpu.make_async_copy(s_v.at[k, s], r_v.at[f], recv_sem.at[PARTS]).start()

        @pl.when(jnp.logical_not(here))
        def _():
            remote(s_v.at[k, s], r_v.at[f], PARTS, (to_z, to_y, x, c)).start()

        return carry

    lax.fori_loop(0, 8, send_parts, 0)
    wait_for(r_v, recv_sem.at[PARTS])

    low = jnp.sum(r_v[...], axis=0)
    update = moments(first_v[...], second_v[...], low)[2]
    spot = y * NT + s
    n_v[spot] = jnp.sum(update * update, axis=0, keepdims=True)
    u_v[f] = update
    for to_y in asides:
        for to_x, to_c in (sides[:-1] if to_y is asides[-1] else sides):
            remote(n_v.at[spot], n_v.at[spot], NEAR, (z, to_y, to_x, to_c)).start()

    def others(do):
        def ring(k, carry):
            do(jnp.where(k >= z, k + 1, k))
            return carry
        lax.fori_loop(0, NZ - 1, ring, 0)

    def send_update(to_z):
        for to_y in asides:
            remote(u_v.at[f], u_v.at[f], UPDATE, (to_z, to_y, x, c)).start()

    others(send_update)
    for to_y in asides[:-1]:
        remote(u_v.at[f], u_v.at[f], UPDATE, (z, to_y, x, c)).start()
    out_ref[32:36] = low
    wait_for(n_v.at[pl.ds(0, NY * NT - 1)], recv_sem.at[NEAR])
    g_v[z] = jnp.sum(n_v[...], axis=0)
    others(lambda to_z: remote(g_v.at[z], g_v.at[z], LINE, (to_z, y, x, c)).start())
    wait_for(u_v.at[pl.ds(0, NF - 1)], recv_sem.at[UPDATE])

    whole = u_v[...].reshape(RANK, DQK)
    high = whole.astype(jnp.bfloat16)
    rest = whole - high.astype(jnp.float32)
    middle = rest.astype(jnp.bfloat16)
    least = (rest - middle.astype(jnp.float32)).astype(jnp.bfloat16)
    basis = b_v[...]
    out_ref[0:32] = (jnp.dot(basis, high, preferred_element_type=jnp.float32)
                     + (jnp.dot(basis, middle, preferred_element_type=jnp.float32)
                        + jnp.dot(basis, least, preferred_element_type=jnp.float32)))
    head_mean = jnp.sum(whole * whole) / (RANK * DQK)

    wait_for(p_v.at[pl.ds(0, NF - 1)], send_sem.at[BASIS])
    for i in range(3):
        wait_for(columns(0), send_sem.at[CROSS + i])
    wait_for(c_v.at[:, pl.ds(0, NX * DQK)], send_sem.at[CORE])

    @pl.when(own)
    def _():
        wait_for(r_v.at[pl.ds(0, NF - 1)], send_sem.at[PARTS])

    @pl.when(jnp.logical_not(own))
    def _():
        wait_for(r_v, send_sem.at[PARTS])

    wait_for(u_v.at[pl.ds(0, NF - 1)], send_sem.at[UPDATE])
    wait_for(n_v.at[pl.ds(0, NY * NT - 1)], send_sem.at[NEAR])
    wait_for(g_v.at[pl.ds(0, NZ - 1)], recv_sem.at[LINE])
    whole_mean = jnp.sum(g_v[...]) / (RANK * HEADS * DQK)
    out_ref[36:40] = jnp.full((4, DQK), head_mean + whole_mean, jnp.float32)
    wait_for(g_v.at[pl.ds(0, NZ - 1)], send_sem.at[LINE])


def finish(sums_ref, master_ref, first_ref, second_ref, step_ref, first_out, second_out, copy_ref):
    factor = 1.0 / jnp.sqrt(sums_ref[36:37])
    step = sums_ref[0:32] * factor
    step_ref[...] = step
    copy_ref[...] = (master_ref[...] + step).astype(jnp.bfloat16)
    first_out[...], second_out[...], _ = moments(first_ref[...], second_ref[...], sums_ref[32:36])


def body(inputs, query_cot, query_basis, query_master, query_first, query_second):
    bf16, f32 = jnp.bfloat16, jnp.float32
    sums = pl.pallas_call(
        kernel,
        out_shape=pltpu.VMEM((40, DQK), f32),
        in_specs=[pl.BlockSpec(memory_space=pl.ANY)] * 5,
        out_specs=pl.BlockSpec(memory_space=pltpu.VMEM),
        scratch_shapes=[
            pltpu.VMEM((256, 2048), bf16),
            pltpu.VMEM((256, NT * DQK), bf16),
            pltpu.VMEM((32, RANK), bf16),
            pltpu.VMEM((4, DQK), f32),
            pltpu.VMEM((4, DQK), f32),
            pltpu.VMEM((NF, 8, 128), bf16),
            pltpu.VMEM((8, NT, 4, DQK), f32),
            pltpu.VMEM((NF, 4, DQK), f32),
            pltpu.VMEM((NF, 4, DQK), f32),
            pltpu.VMEM((NY * NT, 1, DQK), f32),
            pltpu.VMEM((NZ, 1, DQK), f32),
            pltpu.SemaphoreType.DMA((5,)),
            pltpu.SemaphoreType.DMA((9,)),
            pltpu.SemaphoreType.DMA((9,)),
        ],
        compiler_params=pltpu.CompilerParams(collective_id=0, has_side_effects=True),
    )(inputs, query_cot, query_basis, query_first, query_second)
    vmem = pl.BlockSpec(memory_space=pltpu.VMEM)
    in_vmem = lambda a: pltpu.with_memory_space_constraint(a, pltpu.VMEM)
    return pl.pallas_call(
        finish,
        out_shape=(jax.ShapeDtypeStruct((32, DQK), f32), jax.ShapeDtypeStruct((4, DQK), f32),
                   jax.ShapeDtypeStruct((4, DQK), f32), jax.ShapeDtypeStruct((32, DQK), bf16)),
        in_specs=[vmem] * 4,
        out_specs=(vmem,) * 4,
    )(in_vmem(sums), in_vmem(query_master), in_vmem(query_first), in_vmem(query_second))


def solution(mesh):
    torus = Mesh(mesh.devices.reshape(NZ, NY, NX, NC), ("z", "y", "x", "c"))
    in_specs = (P(FS, None), P(FS, TP), P(FS, None), P(FS, TP), P(FS, TP), P(FS, TP))
    out_specs = (P(FS, TP), P(FS, TP), P(FS, TP), P(FS, TP))
    return jax.shard_map(body, mesh=torus, in_specs=in_specs, out_specs=out_specs, check_vma=False)
```

time: 57.9 us -> 51.9 us (0.90)
  other arithmetic: 2.62 us -> 0 us
  Pallas kernels: 52.9 us -> 51.1 us
  local copies, waits for them, and re-layouts: 1.38 us -> 0.01 us
    pallas_call x1 -> x2, Pallas kernels: 52.9 us -> 51.1 us  [the longest x1 50.4 us: body(): pl.pallas_call(kernel, out_shape=pltpu.VMEM((40, DQK), f32), in_specs=[pl...]
    convert_element_type x1 -> x0, other arithmetic: 1.34 us -> none  [body(): copy_q = (query_master + step_q).astype(bf16)]
    add x1 -> x0, other arithmetic: 1.27 us -> none  [moments(): second_new = 0.9 * second + 0.1 * low_grad * low_grad]
    mul x1 -> x0, local copies, waits for them, and re-layouts: 0.69 us -> none  [body(): step_q = out[0:32] * factor]
    unnamed x6, local copies, waits for them, and re-layouts: 0.69 us -> 0.01 us
where the time goes in v2:
time: 51.9 us; the launch traced here: 51.8 us
  Pallas kernels  51.1 us (98%)
  between operations  0.69 us (1%)
    pallas_call x1, Pallas kernels, body(): pl.pallas_call(kernel, out_shape=pltpu.VMEM((40, DQK), f32), in_specs=[pl...  50.4 us

profile of v2, /device:TPU:1, one launch (start us, length us, event | category | flops | bytes accessed | tf_op | source)
XLA Modules:
  0.0 51.8 jit_solution(12614318931999886059)
XLA Ops:
  0.6 0.0 copy-start.2
  0.6 0.0 copy-start.1
  0.7 0.0 copy-start
  0.7 50.4 %shard_map.93.sums_ref = f32[40,128]{1,0:T(8,128)S(1)} custom-call(bf16[256,2048]{1,0:T(8,128)(2,1)} %x_hbm.1, bf16[256,128]{1,0:T(8,128)(2,1)} %c_hbm.1, bf16[32,256]{1,0:T(8,128)(2,1)} %b_hbm.1, f32[4,128]{1,0:T(4,128)} %first_ref.1, f32[4,128]{1,0:T(4,128)} %second_ref.1), custom_call_target="tpu_custom_call" | custom-call | tf_op jit(solution)/shard_map/pallas_call | solution.py:209
  51.1 0.0 copy-done.2
  51.1 0.0 copy-done.1
  51.1 0.0 copy-done
  51.1 0.6 %shard_map.94 = (f32[32,128]{1,0:T(8,128)}, f32[4,128]{1,0:T(4,128)}, f32[4,128]{1,0:T(4,128)}, bf16[32,128]{1,0:T(8,128)(2,1)}) custom-call(f32[40,128]{1,0:T(8,128)S(1)} %shard_map.93.sums_ref, f32[32,128]{1,0:T(8,128)S(1)} %copy-done, f32[4,128]{1,0:T(4,128)S(1)} %copy-done.1, f32[4,128]{1,0:T(4,128)S(1)} %copy-done.2), custom_call_target="tpu_custom_call" | custom-call | tf_op jit(solution)/shard_map/pallas_call | solution.py:234
Async XLA Ops:
  0.6 50.5 %copy-start.2 = (f32[4,128]{1,0:T(4,128)S(1)}, f32[4,128]{1,0:T(4,128)}, u32[]{:S(2)}) copy-start(f32[4,128]{1,0:T(4,128)} %second_ref.1) | copy-start | bytes 6148
  0.6 50.5 %copy-start.1 = (f32[4,128]{1,0:T(4,128)S(1)}, f32[4,128]{1,0:T(4,128)}, u32[]{:S(2)}) copy-start(f32[4,128]{1,0:T(4,128)} %first_ref.1) | copy-start | bytes 6148
  0.7 50.5 %copy-start = (f32[32,128]{1,0:T(8,128)S(1)}, f32[32,128]{1,0:T(8,128)}, u32[]{:S(2)}) copy-start(f32[32,128]{1,0:T(8,128)} %master_ref.1) | copy-start | bytes 49156

commit v3 on v2

--- a/solution.py
+++ b/solution.py
@@ -14,7 +14,7 @@
 TP = ("x", "c")
 FS = ("z", "y")
 MESH = pl.DeviceIdType.MESH
-BASIS, UPDATE, PARTS, NEAR, LINE, CORE, CROSS = 0, 1, 2, 3, 4, 5, 6
+BASIS, UPDATE, PARTS, NEAR, LINE, MOMENTS, LOW, CORE, CROSS = 0, 1, 2, 3, 4, 5, 6, 7, 8
 Y_ORDER = (2, 1, 3, 0)
 
 
@@ -25,7 +25,7 @@
 
 
 def kernel(x_hbm, c_hbm, b_hbm, first_hbm, second_hbm, out_ref,
-           x_v, c_v, b_v, first_v, second_v, p_v, s_v, r_v, u_v, n_v, g_v,
+           x_v, c_v, b_v, own_v, for_v, new_v, p_v, s_v, r_v, u_v, n_v, g_v, l_v,
            local_sem, send_sem, recv_sem):
     z, y, x, c = (lax.axis_index(a) for a in ("z", "y", "x", "c"))
     f, s = z * NY + y, x * NC + c
@@ -63,15 +63,27 @@
         return c_v.at[:, pl.ds(pl.multiple_of(t * DQK, DQK), DQK)]
 
     loads = [pltpu.make_async_copy(src, dst, local_sem.at[i]) for i, (src, dst) in enumerate((
-        (b_hbm, b_v), (c_hbm, columns(s)), (x_hbm, x_v), (first_hbm, first_v), (second_hbm, second_v)))]
+        (b_hbm, b_v), (c_hbm, columns(s)), (x_hbm, x_v), (first_hbm, own_v.at[0]), (second_hbm, own_v.at[1])))]
     for load in loads:
         load.start()
 
+    def block(at_z, at_y):
+        turned = lax.rem(at_z + 2, NZ)
+        to_x = lax.rem(x + 6 - lax.div(turned, 4), NX)
+        return 2 * lax.rem(turned, 4) + lax.div(at_y, 2), to_x, lax.rem(at_y, 2)
+
+    sum_k, sum_x, sum_c = block(z, y)
+    sum_f = 8 * s + sum_k
+    client = (lax.div(sum_f, NY), lax.rem(sum_f, NY), sum_x, sum_c)
+    its_s, its_k = lax.div(f, 8), lax.rem(f, 8)
+    its_x = lax.div(its_s, NC)
+    its_turned = 4 * lax.rem(its_x + 6 - x, NX) + lax.div(its_k, 2)
+    server = (lax.rem(its_turned + 14, NZ), 2 * lax.rem(its_k, 2) + c, its_x, lax.rem(its_s, NC))
+    alone = jnp.logical_and(jnp.logical_and(server[0] == z, server[1] == y), its_s == s)
+
     lane = lax.broadcasted_iota(jnp.int32, (RANK, 128), 1)
     row = lax.broadcasted_iota(jnp.int32, (RANK, 128), 0)
-    slot = lane & 31
-    to_z = 2 * (slot >> 2) + c
-    chosen = row == 16 * to_z + 4 * ((to_z + x) & 3) + (slot & 3)
+    chosen = row == 32 * s + (lane & 31)
     select = jnp.where(chosen, 1.0, 0.0).astype(jnp.bfloat16)
     group = lax.broadcasted_iota(jnp.int32, (8, 128), 1) >> 5
     loads[0].wait()
@@ -94,6 +106,16 @@
         came = columns(lax.rem(x + NX - (2, 1, 3)[i], NX) * NC + c)
         wait_for(came, recv_sem.at[CROSS + i])
         remote(came, came, CORE, partner).start()
+    wait_for(c_v.at[:, pl.ds(0, NX * DQK)], recv_sem.at[CORE])
+
+    @pl.when(alone)
+    def _():
+        pltpu.make_async_copy(own_v, for_v, recv_sem.at[MOMENTS]).start()
+
+    @pl.when(jnp.logical_not(alone))
+    def _():
+        remote(own_v, for_v, MOMENTS, server).start()
+
     wait_for(p_v.at[pl.ds(0, NF - 1)], recv_sem.at[BASIS])
 
     blocks = p_v[...].astype(jnp.float32)
@@ -105,42 +127,38 @@
     high = proj.astype(jnp.bfloat16)
     rest = (proj - high.astype(jnp.float32)).astype(jnp.bfloat16)
     both = jnp.concatenate([high, rest], axis=0)
-    wait_for(c_v.at[:, pl.ds(0, NX * DQK)], recv_sem.at[CORE])
     part = jnp.dot(both, c_v[...], preferred_element_type=jnp.float32)
     part = part[:32] + part[32:]
     for k in range(8):
         for t in range(NT):
             s_v[k, t] = part[4 * k : 4 * k + 4, DQK * t : DQK * (t + 1)]
 
-    own = jnp.logical_and(lax.rem(z, 2) == c, lax.rem(z + x, NY) == y)
-
-    def send_parts(j, carry):
-        h = lax.div(j + 1, 2)
-        k = lax.rem(lax.div(z, 2) + 4 + h * (1 - 2 * lax.rem(j, 2)), 8)
-        to_z = 2 * k + c
-        to_y = lax.rem(to_z + x, NY)
-        for t, (to_x, to_c) in zip(places[:-1], sides):
-            remote(s_v.at[k, t], r_v.at[f], PARTS, (to_z, to_y, to_x, to_c)).start()
-        here = jnp.logical_and(to_z == z, to_y == y)
-
-        @pl.when(here)
-        def _():
-            pltpu.make_async_copy(s_v.at[k, s], r_v.at[f], recv_sem.at[PARTS]).start()
-
-        @pl.when(jnp.logical_not(here))
-        def _():
-            remote(s_v.at[k, s], r_v.at[f], PARTS, (to_z, to_y, x, c)).start()
-
+    low_bits = [(lax.div(to_y, 2), lax.rem(to_y, 2)) for to_y in asides]
+
+    def parts_ring(n, carry):
+        h = lax.div(n + 1, 2)
+        to_z = lax.rem(z + 8 + h * (1 - 2 * lax.rem(n, 2)), NZ)
+        turned = lax.rem(to_z + 2, NZ)
+        to_k = 2 * lax.rem(turned, 4)
+        to_t = NC * lax.rem(x + 6 - lax.div(turned, 4), NX)
+        for to_y, (to_half, to_c) in zip(asides, low_bits):
+            remote(s_v.at[to_k + to_half, to_t + to_c], r_v.at[f], PARTS, (to_z, to_y, x, c)).start()
         return carry
 
-    lax.fori_loop(0, 8, send_parts, 0)
+    lax.fori_loop(0, NZ - 1, parts_ring, 0)
+    for to_y in asides[:-1]:
+        k, to_x, to_c = block(z, to_y)
+        remote(s_v.at[k, to_x * NC + to_c], r_v.at[f], PARTS, (z, to_y, x, c)).start()
+    pltpu.make_async_copy(s_v.at[sum_k, sum_x * NC + sum_c], r_v.at[f], recv_sem.at[PARTS]).start()
+    wait_for(for_v, recv_sem.at[MOMENTS])
     wait_for(r_v, recv_sem.at[PARTS])
 
     low = jnp.sum(r_v[...], axis=0)
-    update = moments(first_v[...], second_v[...], low)[2]
+    update = moments(for_v[0], for_v[1], low)[2]
     spot = y * NT + s
     n_v[spot] = jnp.sum(update * update, axis=0, keepdims=True)
-    u_v[f] = update
+    new_v[0] = update
+    new_v[1] = low
     for to_y in asides:
         for to_x, to_c in (sides[:-1] if to_y is asides[-1] else sides):
             remote(n_v.at[spot], n_v.at[spot], NEAR, (z, to_y, to_x, to_c)).start()
@@ -153,16 +171,33 @@
 
     def send_update(to_z):
         for to_y in asides:
-            remote(u_v.at[f], u_v.at[f], UPDATE, (to_z, to_y, x, c)).start()
+            remote(new_v.at[0], u_v.at[sum_f], UPDATE, (to_z, to_y, sum_x, sum_c)).start()
 
     others(send_update)
     for to_y in asides[:-1]:
-        remote(u_v.at[f], u_v.at[f], UPDATE, (z, to_y, x, c)).start()
-    out_ref[32:36] = low
+        remote(new_v.at[0], u_v.at[sum_f], UPDATE, (z, to_y, sum_x, sum_c)).start()
+    home = jnp.logical_and(sum_x == x, sum_c == c)
+
+    @pl.when(home)
+    def _():
+        pltpu.make_async_copy(new_v.at[0], u_v.at[sum_f], recv_sem.at[UPDATE]).start()
+
+    @pl.when(jnp.logical_not(home))
+    def _():
+        remote(new_v.at[0], u_v.at[sum_f], UPDATE, (z, y, sum_x, sum_c)).start()
+
+    @pl.when(alone)
+    def _():
+        pltpu.make_async_copy(new_v.at[1], l_v, recv_sem.at[LOW]).start()
+
+    @pl.when(jnp.logical_not(alone))
+    def _():
+        remote(new_v.at[1], l_v, LOW, client).start()
+
     wait_for(n_v.at[pl.ds(0, NY * NT - 1)], recv_sem.at[NEAR])
     g_v[z] = jnp.sum(n_v[...], axis=0)
     others(lambda to_z: remote(g_v.at[z], g_v.at[z], LINE, (to_z, y, x, c)).start())
-    wait_for(u_v.at[pl.ds(0, NF - 1)], recv_sem.at[UPDATE])
+    wait_for(u_v, recv_sem.at[UPDATE])
 
     whole = u_v[...].reshape(RANK, DQK)
     high = whole.astype(jnp.bfloat16)
@@ -180,15 +215,23 @@
         wait_for(columns(0), send_sem.at[CROSS + i])
     wait_for(c_v.at[:, pl.ds(0, NX * DQK)], send_sem.at[CORE])
 
-    @pl.when(own)
-    def _():
-        wait_for(r_v.at[pl.ds(0, NF - 1)], send_sem.at[PARTS])
-
-    @pl.when(jnp.logical_not(own))
-    def _():
-        wait_for(r_v, send_sem.at[PARTS])
-
-    wait_for(u_v.at[pl.ds(0, NF - 1)], send_sem.at[UPDATE])
+    wait_for(r_v.at[pl.ds(0, NF - 1)], send_sem.at[PARTS])
+
+    @pl.when(home)
+    def _():
+        wait_for(u_v.at[pl.ds(0, NF - 1)], send_sem.at[UPDATE])
+
+    @pl.when(jnp.logical_not(home))
+    def _():
+        wait_for(u_v, send_sem.at[UPDATE])
+
+    @pl.when(jnp.logical_not(alone))
+    def _():
+        wait_for(own_v, send_sem.at[MOMENTS])
+        wait_for(l_v, send_sem.at[LOW])
+
+    wait_for(l_v, recv_sem.at[LOW])
+    out_ref[32:36] = l_v[...]
     wait_for(n_v.at[pl.ds(0, NY * NT - 1)], send_sem.at[NEAR])
     wait_for(g_v.at[pl.ds(0, NZ - 1)], recv_sem.at[LINE])
     whole_mean = jnp.sum(g_v[...]) / (RANK * HEADS * DQK)
@@ -215,17 +258,19 @@
             pltpu.VMEM((256, 2048), bf16),
             pltpu.VMEM((256, NT * DQK), bf16),
             pltpu.VMEM((32, RANK), bf16),
-            pltpu.VMEM((4, DQK), f32),
-            pltpu.VMEM((4, DQK), f32),
+            pltpu.VMEM((2, 4, DQK), f32),
+            pltpu.VMEM((2, 4, DQK), f32),
+            pltpu.VMEM((2, 4, DQK), f32),
             pltpu.VMEM((NF, 8, 128), bf16),
             pltpu.VMEM((8, NT, 4, DQK), f32),
             pltpu.VMEM((NF, 4, DQK), f32),
             pltpu.VMEM((NF, 4, DQK), f32),
             pltpu.VMEM((NY * NT, 1, DQK), f32),
             pltpu.VMEM((NZ, 1, DQK), f32),
+            pltpu.VMEM((4, DQK), f32),
             pltpu.SemaphoreType.DMA((5,)),
-            pltpu.SemaphoreType.DMA((9,)),
-            pltpu.SemaphoreType.DMA((9,)),
+            pltpu.SemaphoreType.DMA((11,)),
+            pltpu.SemaphoreType.DMA((11,)),
         ],
         compiler_params=pltpu.CompilerParams(collective_id=0, has_side_effects=True),
     )(inputs, query_cot, query_basis, query_first, query_second)

time: 51.9 us -> 50.5 us (0.973)
  Pallas kernels: 51.1 us -> 49.6 us
    pallas_call x1, Pallas kernels: 50.4 us -> 49 us  [body(): pl.pallas_call(kernel, out_shape=pltpu.VMEM((40, DQK), f32), in_specs=[pl...]
where the time goes in v3:
time: 50.5 us; the launch traced here: 50.3 us
  Pallas kernels  49.6 us (98%)
  between operations  0.69 us (1%)
    pallas_call x1, Pallas kernels, body(): pl.pallas_call(kernel, out_shape=pltpu.VMEM((40, DQK), f32), in_specs=[pl...  49 us

profile of v3, /device:TPU:1, one launch (start us, length us, event | category | flops | bytes accessed | tf_op | source)
XLA Modules:
  0.0 50.3 jit_solution(951741889339986444)
XLA Ops:
  0.6 0.0 copy-start.2
  0.6 0.0 copy-start.1
  0.7 0.0 copy-start
  0.7 49.0 %shard_map.93.sums_ref = f32[40,128]{1,0:T(8,128)S(1)} custom-call(bf16[256,2048]{1,0:T(8,128)(2,1)} %x_hbm.1, bf16[256,128]{1,0:T(8,128)(2,1)} %c_hbm.1, bf16[32,256]{1,0:T(8,128)(2,1)} %b_hbm.1, f32[4,128]{1,0:T(4,128)} %first_ref.1, f32[4,128]{1,0:T(4,128)} %second_ref.1), custom_call_target="tpu_custom_call" | custom-call | tf_op jit(solution)/shard_map/pallas_call | solution.py:252
  49.6 0.0 copy-done.2
  49.6 0.0 copy-done.1
  49.6 0.0 copy-done
  49.7 0.6 %shard_map.94 = (f32[32,128]{1,0:T(8,128)}, f32[4,128]{1,0:T(4,128)}, f32[4,128]{1,0:T(4,128)}, bf16[32,128]{1,0:T(8,128)(2,1)}) custom-call(f32[40,128]{1,0:T(8,128)S(1)} %shard_map.93.sums_ref, f32[32,128]{1,0:T(8,128)S(1)} %copy-done, f32[4,128]{1,0:T(4,128)S(1)} %copy-done.1, f32[4,128]{1,0:T(4,128)S(1)} %copy-done.2), custom_call_target="tpu_custom_call" | custom-call | tf_op jit(solution)/shard_map/pallas_call | solution.py:279
Async XLA Ops:
  0.6 49.0 %copy-start.2 = (f32[4,128]{1,0:T(4,128)S(1)}, f32[4,128]{1,0:T(4,128)}, u32[]{:S(2)}) copy-start(f32[4,128]{1,0:T(4,128)} %second_ref.1) | copy-start | bytes 6148
  0.6 49.0 %copy-start.1 = (f32[4,128]{1,0:T(4,128)S(1)}, f32[4,128]{1,0:T(4,128)}, u32[]{:S(2)}) copy-start(f32[4,128]{1,0:T(4,128)} %first_ref.1) | copy-start | bytes 6148
  0.7 49.0 %copy-start = (f32[32,128]{1,0:T(8,128)S(1)}, f32[32,128]{1,0:T(8,128)}, u32[]{:S(2)}) copy-start(f32[32,128]{1,0:T(8,128)} %master_ref.1) | copy-start | bytes 49156

commit v4 on v3

--- a/solution.py
+++ b/solution.py
@@ -155,13 +155,11 @@
 
     low = jnp.sum(r_v[...], axis=0)
     update = moments(for_v[0], for_v[1], low)[2]
-    spot = y * NT + s
+    spot = s
     n_v[spot] = jnp.sum(update * update, axis=0, keepdims=True)
     new_v[0] = update
     new_v[1] = low
-    for to_y in asides:
-        for to_x, to_c in (sides[:-1] if to_y is asides[-1] else sides):
-            remote(n_v.at[spot], n_v.at[spot], NEAR, (z, to_y, to_x, to_c)).start()
+    to_tp(lambda peer: remote(n_v.at[spot], n_v.at[spot], NEAR, peer).start())
 
     def others(do):
         def ring(k, carry):
@@ -194,9 +192,16 @@
     def _():
         remote(new_v.at[1], l_v, LOW, client).start()
 
-    wait_for(n_v.at[pl.ds(0, NY * NT - 1)], recv_sem.at[NEAR])
-    g_v[z] = jnp.sum(n_v[...], axis=0)
-    others(lambda to_z: remote(g_v.at[z], g_v.at[z], LINE, (to_z, y, x, c)).start())
+    wait_for(n_v.at[pl.ds(0, NT - 1)], recv_sem.at[NEAR])
+    g_v[f] = jnp.sum(n_v[...], axis=0)
+
+    def send_sum(to_z):
+        for to_y in asides:
+            remote(g_v.at[f], g_v.at[f], LINE, (to_z, to_y, x, c)).start()
+
+    others(send_sum)
+    for to_y in asides[:-1]:
+        remote(g_v.at[f], g_v.at[f], LINE, (z, to_y, x, c)).start()
     wait_for(u_v, recv_sem.at[UPDATE])
 
     whole = u_v[...].reshape(RANK, DQK)
@@ -232,11 +237,11 @@
 
     wait_for(l_v, recv_sem.at[LOW])
     out_ref[32:36] = l_v[...]
-    wait_for(n_v.at[pl.ds(0, NY * NT - 1)], send_sem.at[NEAR])
-    wait_for(g_v.at[pl.ds(0, NZ - 1)], recv_sem.at[LINE])
+    wait_for(n_v.at[pl.ds(0, NT - 1)], send_sem.at[NEAR])
+    wait_for(g_v.at[pl.ds(0, NF - 1)], recv_sem.at[LINE])
     whole_mean = jnp.sum(g_v[...]) / (RANK * HEADS * DQK)
     out_ref[36:40] = jnp.full((4, DQK), head_mean + whole_mean, jnp.float32)
-    wait_for(g_v.at[pl.ds(0, NZ - 1)], send_sem.at[LINE])
+    wait_for(g_v.at[pl.ds(0, NF - 1)], send_sem.at[LINE])
 
 
 def finish(sums_ref, master_ref, first_ref, second_ref, step_ref, first_out, second_out, copy_ref):
@@ -265,8 +270,8 @@
             pltpu.VMEM((8, NT, 4, DQK), f32),
             pltpu.VMEM((NF, 4, DQK), f32),
             pltpu.VMEM((NF, 4, DQK), f32),
-            pltpu.VMEM((NY * NT, 1, DQK), f32),
-            pltpu.VMEM((NZ, 1, DQK), f32),
+            pltpu.VMEM((NT, 1, DQK), f32),
+            pltpu.VMEM((NF, 1, DQK), f32),
             pltpu.VMEM((4, DQK), f32),
             pltpu.SemaphoreType.DMA((5,)),
             pltpu.SemaphoreType.DMA((11,)),

time: 50.5 us -> 50.5 us (level)
  no operation moved by 1% of the time
where the time goes in v4:
time: 50.5 us; the launch traced here: 50.3 us
  Pallas kernels  49.6 us (98%)
  between operations  0.69 us (1%)
    pallas_call x1, Pallas kernels, body(): pl.pallas_call(kernel, out_shape=pltpu.VMEM((40, DQK), f32), in_specs=[pl...  49 us

profile of v4, /device:TPU:1, one launch (start us, length us, event | category | flops | bytes accessed | tf_op | source)
XLA Modules:
  0.0 50.3 jit_solution(1846756525258091597)
XLA Ops:
  0.6 0.0 copy-start.2
  0.6 0.0 copy-start.1
  0.7 0.0 copy-start
  0.7 49.0 %shard_map.93.sums_ref = f32[40,128]{1,0:T(8,128)S(1)} custom-call(bf16[256,2048]{1,0:T(8,128)(2,1)} %x_hbm.1, bf16[256,128]{1,0:T(8,128)(2,1)} %c_hbm.1, bf16[32,256]{1,0:T(8,128)(2,1)} %b_hbm.1, f32[4,128]{1,0:T(4,128)} %first_ref.1, f32[4,128]{1,0:T(4,128)} %second_ref.1), custom_call_target="tpu_custom_call" | custom-call | tf_op jit(solution)/shard_map/pallas_call | solution.py:257
  49.6 0.0 copy-done.2
  49.7 0.0 copy-done.1
  49.7 0.0 copy-done
  49.7 0.6 %shard_map.94 = (f32[32,128]{1,0:T(8,128)}, f32[4,128]{1,0:T(4,128)}, f32[4,128]{1,0:T(4,128)}, bf16[32,128]{1,0:T(8,128)(2,1)}) custom-call(f32[40,128]{1,0:T(8,128)S(1)} %shard_map.93.sums_ref, f32[32,128]{1,0:T(8,128)S(1)} %copy-done, f32[4,128]{1,0:T(4,128)S(1)} %copy-done.1, f32[4,128]{1,0:T(4,128)S(1)} %copy-done.2), custom_call_target="tpu_custom_call" | custom-call | tf_op jit(solution)/shard_map/pallas_call | solution.py:284
Async XLA Ops:
  0.6 49.0 %copy-start.2 = (f32[4,128]{1,0:T(4,128)S(1)}, f32[4,128]{1,0:T(4,128)}, u32[]{:S(2)}) copy-start(f32[4,128]{1,0:T(4,128)} %second_ref.1) | copy-start | bytes 6148
  0.6 49.0 %copy-start.1 = (f32[4,128]{1,0:T(4,128)S(1)}, f32[4,128]{1,0:T(4,128)}, u32[]{:S(2)}) copy-start(f32[4,128]{1,0:T(4,128)} %first_ref.1) | copy-start | bytes 6148
  0.7 49.0 %copy-start = (f32[32,128]{1,0:T(8,128)S(1)}, f32[32,128]{1,0:T(8,128)}, u32[]{:S(2)}) copy-start(f32[32,128]{1,0:T(8,128)} %master_ref.1) | copy-start | bytes 49156

commit v5 on v3

--- a/solution.py
+++ b/solution.py
@@ -196,7 +196,15 @@
 
     wait_for(n_v.at[pl.ds(0, NY * NT - 1)], recv_sem.at[NEAR])
     g_v[z] = jnp.sum(n_v[...], axis=0)
-    others(lambda to_z: remote(g_v.at[z], g_v.at[z], LINE, (to_z, y, x, c)).start())
+
+    @pl.when(c == 1)
+    def _():
+        def both_cores(to_z):
+            for to_c in (0, 1):
+                remote(g_v.at[z], g_v.at[z], LINE, (to_z, y, x, to_c)).start()
+
+        others(both_cores)
+
     wait_for(u_v, recv_sem.at[UPDATE])
 
     whole = u_v[...].reshape(RANK, DQK)
@@ -236,7 +244,10 @@
     wait_for(g_v.at[pl.ds(0, NZ - 1)], recv_sem.at[LINE])
     whole_mean = jnp.sum(g_v[...]) / (RANK * HEADS * DQK)
     out_ref[36:40] = jnp.full((4, DQK), head_mean + whole_mean, jnp.float32)
-    wait_for(g_v.at[pl.ds(0, NZ - 1)], send_sem.at[LINE])
+
+    @pl.when(c == 1)
+    def _():
+        wait_for(n_v.at[pl.ds(0, 2 * (NZ - 1))], send_sem.at[LINE])
 
 
 def finish(sums_ref, master_ref, first_ref, second_ref, step_ref, first_out, second_out, copy_ref):

time: 50.5 us -> 50.5 us (level)
  no operation moved by 1% of the time
where the time goes in v5:
time: 50.5 us; the launch traced here: 50.3 us
  Pallas kernels  49.6 us (98%)
  between operations  0.69 us (1%)
    pallas_call x1, Pallas kernels, body(): pl.pallas_call(kernel, out_shape=pltpu.VMEM((40, DQK), f32), in_specs=[pl...  49 us

profile of v5, /device:TPU:1, one launch (start us, length us, event | category | flops | bytes accessed | tf_op | source)
XLA Modules:
  0.0 50.3 jit_solution(8410901671170358399)
XLA Ops:
  0.6 0.0 copy-start.2
  0.6 0.0 copy-start.1
  0.7 0.0 copy-start
  0.7 49.0 %shard_map.93.sums_ref = f32[40,128]{1,0:T(8,128)S(1)} custom-call(bf16[256,2048]{1,0:T(8,128)(2,1)} %x_hbm.1, bf16[256,128]{1,0:T(8,128)(2,1)} %c_hbm.1, bf16[32,256]{1,0:T(8,128)(2,1)} %b_hbm.1, f32[4,128]{1,0:T(4,128)} %first_ref.1, f32[4,128]{1,0:T(4,128)} %second_ref.1), custom_call_target="tpu_custom_call" | custom-call | tf_op jit(solution)/shard_map/pallas_call | solution.py:263
  49.6 0.0 copy-done.2
  49.6 0.0 copy-done.1
  49.6 0.0 copy-done
  49.7 0.6 %shard_map.94 = (f32[32,128]{1,0:T(8,128)}, f32[4,128]{1,0:T(4,128)}, f32[4,128]{1,0:T(4,128)}, bf16[32,128]{1,0:T(8,128)(2,1)}) custom-call(f32[40,128]{1,0:T(8,128)S(1)} %shard_map.93.sums_ref, f32[32,128]{1,0:T(8,128)S(1)} %copy-done, f32[4,128]{1,0:T(4,128)S(1)} %copy-done.1, f32[4,128]{1,0:T(4,128)S(1)} %copy-done.2), custom_call_target="tpu_custom_call" | custom-call | tf_op jit(solution)/shard_map/pallas_call | solution.py:290
Async XLA Ops:
  0.6 49.0 %copy-start.2 = (f32[4,128]{1,0:T(4,128)S(1)}, f32[4,128]{1,0:T(4,128)}, u32[]{:S(2)}) copy-start(f32[4,128]{1,0:T(4,128)} %second_ref.1) | copy-start | bytes 6148
  0.6 49.0 %copy-start.1 = (f32[4,128]{1,0:T(4,128)S(1)}, f32[4,128]{1,0:T(4,128)}, u32[]{:S(2)}) copy-start(f32[4,128]{1,0:T(4,128)} %first_ref.1) | copy-start | bytes 6148
  0.7 49.0 %copy-start = (f32[32,128]{1,0:T(8,128)S(1)}, f32[32,128]{1,0:T(8,128)}, u32[]{:S(2)}) copy-start(f32[32,128]{1,0:T(8,128)} %master_ref.1) | copy-start | bytes 49156
